TPU v7x, 32 devices: a whole 2x2x4 slice. The times are simulated.
32 devices in a mesh: fs: 8 (over z, y), tp: 4 (over x, core).
Axes of the slice: x: 2, y: 2, z: 4, core: 2. Of those that a mesh axis runs over, the one named last changes fastest.
Arguments:
- inputs: bfloat16 [2048, 2048], P('fs', 'tp'), may hold values from -6 to 6
- cotangent: bfloat16 [2048, 2048], P('fs', 'tp'), may hold values from -8 to 8
- gate_weight: bfloat16 [2048, 5632], P('fs', 'tp'), may hold values from -0.125 to 0.125
- up_weight: bfloat16 [2048, 5632], P('fs', 'tp'), may hold values from -0.125 to 0.125
- down_weight: bfloat16 [5632, 2048], P('tp', 'fs'), may hold values from -0.078125 to 0.078125
Outputs:
- grad_inputs: bfloat16 [2048, 2048], P('fs', 'tp')
- grad_gate: float32 [2048, 5632], P('fs', 'tp')
- grad_up: float32 [2048, 5632], P('fs', 'tp')
- grad_down: float32 [5632, 2048], P('tp', 'fs')
All inputs are finite; a program needn't handle non-finite values.
Results may differ from a plain program's by a relative error of at most 0.015.
Values may be sent and summed in bfloat16 or wider, within the bound.
A program may use at most 64 MiB of HBM per device.

v0:
```python
import jax
import jax.numpy as jnp
from jax import lax
from jax.sharding import PartitionSpec as P


def contract_rows(left, right):
    return lax.dot_general(
        left, right, (((0,), (0,)), ((), ())), preferred_element_type=jnp.float32
    )


def contract_cols(left, right):
    return lax.dot_general(
        left, right, (((1,), (1,)), ((), ())), preferred_element_type=jnp.float32
    )


def per_device(inputs, cotangent, gate_weight, up_weight, down_weight):
    whole_inputs, whole_cotangent = (
        lax.all_gather(inputs, "tp", axis=1, tiled=True),
        lax.all_gather(cotangent, "tp", axis=1, tiled=True),
    )
    gate_whole, up_whole = (
        lax.all_gather(gate_weight, "fs", axis=0, tiled=True),
        lax.all_gather(up_weight, "fs", axis=0, tiled=True),
    )
    gate_pre = jnp.dot(whole_inputs, gate_whole, preferred_element_type=jnp.float32)
    up_pre = jnp.dot(whole_inputs, up_whole, preferred_element_type=jnp.float32)
    gate_sig = jax.nn.sigmoid(gate_pre)
    gate_act = gate_pre * gate_sig
    hidden = (gate_act * up_pre).astype(jnp.bfloat16)
    grad_hidden = contract_cols(
        whole_cotangent, lax.all_gather(down_weight, "fs", axis=1, tiled=True)
    )
    grad_gate_pre = (grad_hidden * up_pre * gate_sig * (1.0 + gate_pre * (1.0 - gate_sig))).astype(
        jnp.bfloat16
    )
    grad_up_pre = (grad_hidden * gate_act).astype(jnp.bfloat16)
    pre_grads = jnp.concatenate([grad_gate_pre, grad_up_pre], axis=1)
    width = gate_weight.shape[1]
    partial_sum = contract_cols(grad_gate_pre, gate_whole) + contract_cols(grad_up_pre, up_whole)
    grad_inputs = lax.psum_scatter(
        partial_sum.astype(jnp.bfloat16), "tp", scatter_dimension=1, tiled=True
    )
    expand = lax.psum_scatter(
        contract_rows(whole_inputs, pre_grads).astype(jnp.bfloat16),
        "fs",
        scatter_dimension=0,
        tiled=True,
    ).astype(jnp.float32)
    down = lax.psum_scatter(
        contract_rows(whole_cotangent, hidden).astype(jnp.bfloat16),
        "fs",
        scatter_dimension=0,
        tiled=True,
    ).astype(jnp.float32)
    grad_gate = expand[:, :width]
    grad_up = expand[:, width:]
    grad_down = down.T
    return (grad_inputs, grad_gate, grad_up, grad_down)


def solution(mesh):
    return jax.shard_map(
        per_device,
        mesh=mesh,
        in_specs=(P("fs", "tp"), P("fs", "tp"), P("fs", "tp"), P("fs", "tp"), P("tp", "fs")),
        out_specs=(P("fs", "tp"), P("fs", "tp"), P("fs", "tp"), P("tp", "fs")),
        check_vma=False,
    )
```

profile of v0, /device:TPU:0, one launch (start us, length us, event | category | flops | bytes accessed | tf_op | source)
XLA Modules:
  0.0 670.5 jit_solution(8997837980882983968)
XLA Ops:
  7.2 0.7 all-gather.10.cloned.1.call-update
  7.9 0.7 all-gather.12.cloned.1.call-update
  8.7 0.7 all-gather.14.cloned.1.call-update
  9.4 0.5 all-gather.6.cloned.1.call-update
  10.0 0.5 all-gather.8.cloned.1.call-update
  10.6 18.4 %all-gather.10.cloned.1.call-done = bf16[256,2048]{1,0:T(8,128)(2,1)} async-done(((bf16[256,512]{1,0:T(8,128)(2,1)}), bf16[256,2048]{1,0:T(8,128)(2,1)}) %all-gather.10.cloned.1.call-update) | async-done | bytes 1048592 | tf_op jit(solution)/shard_map/all_gather | solution.py:21
  29.0 94.5 %all-gather.12.cloned.1.call-done = bf16[2048,1408]{1,0:T(8,128)(2,1)} async-done(((bf16[256,1408]{1,0:T(8,128)(2,1)}), bf16[2048,1408]{1,0:T(8,128)(2,1)}) %all-gather.12.cloned.1.call-update) | async-done | bytes 5767184 | tf_op jit(solution)/shard_map/all_gather | solution.py:26
  123.5 4.8 fusion.10
  128.3 87.9 %all-gather.14.cloned.1.call-done = bf16[2048,1408]{1,0:T(8,128)(2,1)} async-done(((bf16[256,1408]{1,0:T(8,128)(2,1)}), bf16[2048,1408]{1,0:T(8,128)(2,1)}) %all-gather.14.cloned.1.call-update) | async-done | bytes 5767184 | tf_op jit(solution)/shard_map/all_gather | solution.py:25
  216.2 5.5 fusion.11
  221.8 10.8 %all-gather.6.cloned.1.call-done = bf16[256,2048]{1,0:T(8,128)(2,1)} async-done(((bf16[256,512]{1,0:T(8,128)(2,1)}), bf16[256,2048]{1,0:T(8,128)(2,1)}) %all-gather.6.cloned.1.call-update) | async-done | bytes 1048592 | tf_op jit(solution)/shard_map/all_gather | solution.py:22
  232.6 5.9 fusion
  238.6 89.1 %all-gather.8.cloned.1.call-done = bf16[1408,2048]{1,0:T(8,128)(2,1)} async-done(((bf16[1408,256]{1,0:T(8,128)(2,1)}), bf16[1408,2048]{1,0:T(8,128)(2,1)}) %all-gather.8.cloned.1.call-update) | async-done | bytes 5767184 | tf_op jit(solution)/shard_map/all_gather | solution.py:34
  327.7 5.6 multiply_convert_fusion.1
  333.3 6.1 convert_bitcast_fusion
  339.6 4.5 fusion.12
  344.1 5.5 fusion.1
  349.6 90.8 %reduce-scatter.8.cloned.1.call-done = bf16[256,1408]{0,1:T(8,128)(2,1)} async-done(((bf16[2048,1408]{0,1:T(8,128)(2,1)}), bf16[256,1408]{0,1:T(8,128)(2,1)}) %reduce-scatter.8.cloned.1.call-update) | async-done | bytes 720912 | tf_op jit(solution)/shard_map/reduce_scatter | solution.py:52
  440.4 2.3 convert_bitcast_fusion.1
  442.8 193.9 %reduce-scatter.6.cloned.1.call-done = bf16[256,2816]{0,1:T(8,128)(2,1)} async-done(((bf16[2048,2816]{0,1:T(8,128)(2,1)}), bf16[256,2816]{0,1:T(8,128)(2,1)}) %reduce-scatter.6.cloned.1.call-update) | async-done | bytes 1441808 | tf_op jit(solution)/shard_map/reduce_scatter | solution.py:46
  636.7 1.5 fusion.9
  638.2 1.5 copy.10
  639.8 1.5 copy.9
  641.3 22.4 %reduce-scatter.4.cloned.1.call-done = bf16[256,512]{1,0:T(8,128)(2,1)} async-done(((bf16[256,2048]{1,0:T(8,128)(2,1)}), bf16[256,512]{1,0:T(8,128)(2,1)}) %reduce-scatter.4.cloned.1.call-update) | async-done | bytes 262160 | tf_op jit(solution)/shard_map/reduce_scatter | solution.py:43
  (17 shorter events, 0.6 us)
Async XLA Ops:
  7.2 21.8 %all-gather.10.cloned.1.call-start = ((), (), s32[]{:S(2)}) async-start(), calls=%async_computation.5 | async-start | bytes 1310720 | tf_op jit(solution)/shard_map/all_gather | solution.py:21
  7.9 115.6 %all-gather.12.cloned.1.call-start = ((), (), s32[]{:S(2)}) async-start(), calls=%async_computation.6 | async-start | bytes 6488064 | tf_op jit(solution)/shard_map/all_gather | solution.py:26
  8.6 207.6 %all-gather.14.cloned.1.call-start = ((), (), s32[]{:S(2)}) async-start(), calls=%async_computation.7 | async-start | bytes 6488064 | tf_op jit(solution)/shard_map/all_gather | solution.py:25
  9.4 223.2 %all-gather.6.cloned.1.call-start = ((), (), s32[]{:S(2)}) async-start(), calls=%async_computation.3 | async-start | bytes 1310720 | tf_op jit(solution)/shard_map/all_gather | solution.py:22
  10.0 317.7 %all-gather.8.cloned.1.call-start = ((), (), s32[]{:S(2)}) async-start(), calls=%async_computation.4 | async-start | bytes 6488064 | tf_op jit(solution)/shard_map/all_gather | solution.py:34
  10.5 429.9 %reduce-scatter.8.cloned.1.call-start = ((), (), s32[]{:S(2)}) async-start(), calls=%async_computation.10 | async-start | bytes 6488064 | tf_op jit(solution)/shard_map/reduce_scatter | solution.py:52
  29.0 187.2 %copy-start = (bf16[256,2048]{1,0:T(8,128)(2,1)S(1)}, bf16[256,2048]{1,0:T(8,128)(2,1)}, u32[]{:S(2)}) copy-start(bf16[256,2048]{1,0:T(8,128)(2,1)} %all-gather.10.cloned.1.call-done) | copy-start | bytes 3145732
  128.3 104.3 %copy-start.2 = (f32[256,1408]{1,0:T(8,128)}, f32[256,1408]{1,0:T(8,128)S(1)}, u32[]{:S(2)}) copy-start(f32[256,1408]{1,0:T(8,128)S(1)} %fusion.10) | copy-start | bytes 4325380
  238.5 89.1 %copy-start.1 = (bf16[256,2048]{1,0:T(8,128)(2,1)S(1)}, bf16[256,2048]{1,0:T(8,128)(2,1)}, u32[]{:S(2)}) copy-start(bf16[256,2048]{1,0:T(8,128)(2,1)} %all-gather.6.cloned.1.call-done) | copy-start | bytes 3145732
  238.6 398.1 %reduce-scatter.6.cloned.1.call-start = ((), (), s32[]{:S(2)}) async-start(), calls=%async_computation.9 | async-start | bytes 12976128 | tf_op jit(solution)/shard_map/reduce_scatter | solution.py:46
  339.4 324.3 %reduce-scatter.4.cloned.1.call-start = ((), (), s32[]{:S(2)}) async-start(), calls=%async_computation.8 | async-start | bytes 1310720 | tf_op jit(solution)/shard_map/reduce_scatter | solution.py:43
Sparse Core Ops, SparseCore 0:
  9.5 19.4 all-gather.9
  31.2 92.2 all-gather.11
  125.7 90.4 all-gather.13
  217.6 14.9 all-gather.5
  234.5 93.1 all-gather.7
  331.2 109.2 reduce-scatter.7
  444.0 192.6 reduce-scatter.5
  639.8 23.8 reduce-scatter.3
where the time goes:
time: 671 us
  waiting for transfers between devices  611 us (91%)
  matrix products  37.9 us (6%)
  between operations  14.2 us (2%)
    reduce_scatter x1, waiting for transfers between devices, per_device(): lax.psum_scatter(contract_rows(whole_inputs, pre_grads).astype(jnp.bfloat...  194 us
    all_gather x1, waiting for transfers between devices, per_device(): lax.all_gather(up_weight, 'fs', axis=0, tiled=True)  94.5 us
    reduce_scatter x1, waiting for transfers between devices, per_device(): lax.psum_scatter(contract_rows(whole_cotangent, hidden).astype(jnp.bfloat...  90.8 us
    all_gather x1, waiting for transfers between devices, per_device(): lax.all_gather(down_weight, 'fs', axis=1, tiled=True)  89.1 us
    all_gather x1, waiting for transfers between devices, per_device(): lax.all_gather(gate_weight, 'fs', axis=0, tiled=True)  87.9 us
    reduce_scatter x1, waiting for transfers between devices, per_device(): lax.psum_scatter(partial_sum.astype(jnp.bfloat16), 'tp', scatter_dimensio...  22.4 us
    all_gather x1, waiting for transfers between devices, per_device(): lax.all_gather(inputs, 'tp', axis=1, tiled=True)  18.4 us
    dot_general x3, matrix products, contract_cols(): lax.dot_general(left, right, (((1,), (1,)), ((), ())), preferred_element_...  15.6 us
  transfers between devices with their start and end apart: 8, of which 8 were waited for; matrix products, arithmetic and copies ran while one was open for 7% of the time, Pallas kernels for 0%

commit v1 on v0

--- a/solution.py
+++ b/solution.py
@@ -31,7 +31,10 @@
     gate_act = gate_pre * gate_sig
     hidden = (gate_act * up_pre).astype(jnp.bfloat16)
     grad_hidden = contract_cols(
-        whole_cotangent, lax.all_gather(down_weight, "fs", axis=1, tiled=True)
+        whole_cotangent,
+        jnp.concatenate(
+            lax.all_to_all(jnp.stack([down_weight] * lax.axis_size("fs")), "fs", 0, 0), axis=1
+        ),
     )
     grad_gate_pre = (grad_hidden * up_pre * gate_sig * (1.0 + gate_pre * (1.0 - gate_sig))).astype(
         jnp.bfloat16

time: 671 us -> 668 us (level)
  waiting for transfers between devices: 611 us -> 597 us
  starting transfers between devices: 0.49 us -> 7.76 us
    all_gather x1 -> x0, waiting for transfers between devices: 89.1 us -> none  [per_device(): lax.all_gather(down_weight, 'fs', axis=1, tiled=True)]
    all_gather x1, waiting for transfers between devices: 94.5 us -> 182 us  [per_device(): lax.all_gather(up_weight, 'fs', axis=0, tiled=True)]
    all_gather x1, waiting for transfers between devices: 18.4 us -> 8.37 us  [per_device(): lax.all_gather(inputs, 'tp', axis=1, tiled=True)]
    all_to_all x0 -> x1, starting transfers between devices: none -> 7.31 us  [per_device(): lax.all_to_all(jnp.stack([down_weight] * lax.axis_size('fs')), 'fs', 0, 0)]
  transfers between devices with their start and end apart: 8 -> 8, of which waited for: 8 -> 7; matrix products, arithmetic and copies ran while one was open for 7% -> 7% of each run, Pallas kernels for 0% -> 0%
where the time goes in v1:
time: 668 us
  waiting for transfers between devices  597 us (89%)
  matrix products  37.7 us (6%)
  between operations  14.2 us (2%)
  local copies, waits for them, and re-layouts  9.07 us (1%)
  starting transfers between devices  7.76 us (1%)
    reduce_scatter x1, waiting for transfers between devices, per_device(): lax.psum_scatter(contract_rows(whole_inputs, pre_grads).astype(jnp.bfloat...  194 us
    all_gather x1, waiting for transfers between devices, per_device(): lax.all_gather(up_weight, 'fs', axis=0, tiled=True)  182 us
    all_gather x1, waiting for transfers between devices, per_device(): lax.all_gather(gate_weight, 'fs', axis=0, tiled=True)  88.6 us
    reduce_scatter x1, waiting for transfers between devices, per_device(): lax.psum_scatter(contract_rows(whole_cotangent, hidden).astype(jnp.bfloat...  88.2 us
    reduce_scatter x1, waiting for transfers between devices, per_device(): lax.psum_scatter(partial_sum.astype(jnp.bfloat16), 'tp', scatter_dimensio...  22.4 us
    dot_general x3, matrix products, contract_cols(): lax.dot_general(left, right, (((1,), (1,)), ((), ())), preferred_element_...  15.4 us
  transfers between devices with their start and end apart: 8, of which 7 were waited for; matrix products, arithmetic and copies ran while one was open for 7% of the time, Pallas kernels for 0%

profile of v1, /device:TPU:0, one launch (start us, length us, event | category | flops | bytes accessed | tf_op | source)
XLA Modules:
  0.0 667.7 jit_solution(977462011852424877)
XLA Ops:
  7.2 0.7 all-gather.7.cloned.1.call-update
  8.0 0.7 all-gather.9.cloned.1.call-update
  8.7 0.7 all-gather.11.cloned.1.call-update
  10.3 2.9 stack.2
  13.3 7.3 %all-to-all-start = ((bf16[8,1408,256]{1,2,0:T(8,128)(2,1)}), bf16[8,1408,256]{1,2,0:T(8,128)(2,1)}, u32[]{:S(2)}, u32[]{:S(2)}) async-start(bf16[8,1408,256]{1,2,0:T(8,128)(2,1)} %stack.2), calls=%async_computation | async-start | bytes 11534336 | tf_op jit(solution)/shard_map/all_to_all | solution.py:36
  20.6 8.4 %all-gather.7.cloned.1.call-done = bf16[256,2048]{1,0:T(8,128)(2,1)} async-done(((bf16[256,512]{1,0:T(8,128)(2,1)}), bf16[256,2048]{1,0:T(8,128)(2,1)}) %all-gather.7.cloned.1.call-update) | async-done | bytes 1048592 | tf_op jit(solution)/shard_map/all_gather | solution.py:21
  29.0 181.9 %all-gather.9.cloned.1.call-done = bf16[2048,1408]{1,0:T(8,128)(2,1)} async-done(((bf16[256,1408]{1,0:T(8,128)(2,1)}), bf16[2048,1408]{1,0:T(8,128)(2,1)}) %all-gather.9.cloned.1.call-update) | async-done | bytes 5767184 | tf_op jit(solution)/shard_map/all_gather | solution.py:26
  210.9 4.8 fusion.10
  215.7 88.6 %all-gather.11.cloned.1.call-done = bf16[2048,1408]{1,0:T(8,128)(2,1)} async-done(((bf16[256,1408]{1,0:T(8,128)(2,1)}), bf16[2048,1408]{1,0:T(8,128)(2,1)}) %all-gather.11.cloned.1.call-update) | async-done | bytes 5767184 | tf_op jit(solution)/shard_map/all_gather | solution.py:25
  304.3 5.5 fusion.11
  309.8 10.8 %all-gather.5.cloned.1.call-done = bf16[256,2048]{1,0:T(8,128)(2,1)} async-done(((bf16[256,512]{1,0:T(8,128)(2,1)}), bf16[256,2048]{1,0:T(8,128)(2,1)}) %all-gather.5.cloned.1.call-update) | async-done | bytes 1048592 | tf_op jit(solution)/shard_map/all_gather | solution.py:22
  320.6 5.9 fusion
  326.6 1.1 copy-done.2
  327.8 5.4 multiply_convert_fusion.1
  333.2 6.1 convert_bitcast_fusion
  339.6 4.5 fusion.12
  344.1 5.5 fusion.1
  349.6 88.2 %reduce-scatter.8.cloned.1.call-done = bf16[256,1408]{0,1:T(8,128)(2,1)} async-done(((bf16[2048,1408]{0,1:T(8,128)(2,1)}), bf16[256,1408]{0,1:T(8,128)(2,1)}) %reduce-scatter.8.cloned.1.call-update) | async-done | bytes 720912 | tf_op jit(solution)/shard_map/reduce_scatter | solution.py:55
  437.8 2.3 convert_bitcast_fusion.1
  440.1 193.7 %reduce-scatter.6.cloned.1.call-done = bf16[256,2816]{0,1:T(8,128)(2,1)} async-done(((bf16[2048,2816]{0,1:T(8,128)(2,1)}), bf16[256,2816]{0,1:T(8,128)(2,1)}) %reduce-scatter.6.cloned.1.call-update) | async-done | bytes 1441808 | tf_op jit(solution)/shard_map/reduce_scatter | solution.py:49
  633.8 1.5 fusion.9
  635.4 1.5 copy.13
  636.9 1.5 copy.12
  638.4 22.4 %reduce-scatter.4.cloned.1.call-done = bf16[256,512]{1,0:T(8,128)(2,1)} async-done(((bf16[256,2048]{1,0:T(8,128)(2,1)}), bf16[256,512]{1,0:T(8,128)(2,1)}) %reduce-scatter.4.cloned.1.call-update) | async-done | bytes 262160 | tf_op jit(solution)/shard_map/reduce_scatter | solution.py:46
  (20 shorter events, 1.4 us)
Async XLA Ops:
  7.2 2.8 copy-start.1
  7.2 21.8 %all-gather.7.cloned.1.call-start = ((), (), s32[]{:S(2)}) async-start(), calls=%async_computation.5 | async-start | bytes 1310720 | tf_op jit(solution)/shard_map/all_gather | solution.py:21
  7.9 203.0 %all-gather.9.cloned.1.call-start = ((), (), s32[]{:S(2)}) async-start(), calls=%async_computation.6 | async-start | bytes 6488064 | tf_op jit(solution)/shard_map/all_gather | solution.py:26
  8.7 295.6 %all-gather.11.cloned.1.call-start = ((), (), s32[]{:S(2)}) async-start(), calls=%async_computation.7 | async-start | bytes 6488064 | tf_op jit(solution)/shard_map/all_gather | solution.py:25
  9.4 311.2 %all-gather.5.cloned.1.call-start = ((), (), s32[]{:S(2)}) async-start(), calls=%async_computation.4 | async-start | bytes 1310720 | tf_op jit(solution)/shard_map/all_gather | solution.py:22
  13.3 313.4 %all-to-all-start = ((bf16[8,1408,256]{1,2,0:T(8,128)(2,1)}), bf16[8,1408,256]{1,2,0:T(8,128)(2,1)}, u32[]{:S(2)}, u32[]{:S(2)}) async-start(bf16[8,1408,256]{1,2,0:T(8,128)(2,1)} %stack.2), calls=%async_computation | async-start | bytes 11534336 | tf_op jit(solution)/shard_map/all_to_all | solution.py:36
  20.6 417.2 %reduce-scatter.8.cloned.1.call-start = ((), (), s32[]{:S(2)}) async-start(), calls=%async_computation.10 | async-start | bytes 6488064 | tf_op jit(solution)/shard_map/reduce_scatter | solution.py:55
  29.0 275.3 %copy-start = (bf16[256,2048]{1,0:T(8,128)(2,1)S(1)}, bf16[256,2048]{1,0:T(8,128)(2,1)}, u32[]{:S(2)}) copy-start(bf16[256,2048]{1,0:T(8,128)(2,1)} %all-gather.7.cloned.1.call-done) | copy-start | bytes 3145732
  215.7 105.0 %copy-start.3 = (f32[256,1408]{1,0:T(8,128)}, f32[256,1408]{1,0:T(8,128)S(1)}, u32[]{:S(2)}) copy-start(f32[256,1408]{1,0:T(8,128)S(1)} %fusion.10) | copy-start | bytes 4325380
  326.6 1.2 copy-start.2
  326.6 307.2 %reduce-scatter.6.cloned.1.call-start = ((), (), s32[]{:S(2)}) async-start(), calls=%async_computation.9 | async-start | bytes 12976128 | tf_op jit(solution)/shard_map/reduce_scatter | solution.py:49
  339.3 321.5 %reduce-scatter.4.cloned.1.call-start = ((), (), s32[]{:S(2)}) async-start(), calls=%async_computation.8 | async-start | bytes 1310720 | tf_op jit(solution)/shard_map/reduce_scatter | solution.py:46
Sparse Core Ops, SparseCore 0:
  9.5 19.4 all-gather.6
  31.2 179.6 all-gather.8
  213.1 91.1 all-gather.10
  305.7 14.9 all-gather.4
  326.7 111.0 reduce-scatter.7
  441.3 192.4 reduce-scatter.5
  636.9 23.8 reduce-scatter.3
